TPU v7x, 32 devices: a whole 2x2x4 slice. The times are simulated.
32 devices in a mesh: sp: 8 (over z, y), tp: 4 (over x, core).
Axes of the slice: x: 2, y: 2, z: 4, core: 2. Of those that a mesh axis runs over, the one named last changes fastest.
Arguments:
- tokens: bfloat16 [3072, 2048], P(('sp', 'tp')), may hold values from -6 to 6
- input_norm_gain: bfloat16 [2048], replicated, may hold values from 0.099609375 to 1.8984375
- output_gate_weight: bfloat16 [2048, 2048], P('sp', 'tp'), may hold values from -0.125 to 0.125
- value_input_weight: bfloat16 [2048, 2048], P('sp', 'tp'), may hold values from -0.125 to 0.125
- recurrence_input_weight: bfloat16 [2048, 2048], P('sp', 'tp'), may hold values from -0.125 to 0.125
- convolution_filter: bfloat16 [3, 2048], P(None, 'tp'), may hold values from -3.5 to 3.5
- recurrence_filter: bfloat16 [4, 2048], P(None, 'tp'), may hold values from -3 to 3
- recurrence_gate_matrix: bfloat16 [8, 256, 256], P('tp'), may hold values from -0.375 to 0.375
- input_gate_matrix: bfloat16 [8, 256, 256], P('tp'), may hold values from -0.375 to 0.375
- channel_decay_rate: float32 [2048], P('tp'), may hold values from 1.6276042e-05 to 0.025
- head_log_decay_add: float32 [8, 3072], P('tp', 'sp'), may hold values from -0.7 to 0
- initial_state: float32 [2048], P('tp'), may hold values from -6 to 6
- output_matrix: bfloat16 [2048, 2048], P(None, 'tp'), may hold values from -0.125 to 0.125
Outputs:
- mixed: bfloat16 [3072, 2048], P(('sp', 'tp'))
All inputs are finite; a program needn't handle non-finite values.
Results may differ from a plain program's by a relative error of at most 0.015.
Values may be sent and summed in bfloat16 or wider, within the bound.
A program may use at most 64 MiB of HBM per device.

v0:
```python
import jax
import jax.numpy as jnp
from jax import lax
from jax.sharding import PartitionSpec as P

DECAY_MULTIPLIER = 8.0
NORM_EPS = 1e-06


def shifted(value, axis, steps):
    count = lax.axis_size(axis)
    first, last = (max(0, -steps), min(count, count - steps))
    return lax.ppermute(value, axis, [(source, source + steps) for source in range(first, last)])


def causal_taps(values, before, tap_weights):
    extended = jnp.concatenate([before, values], axis=0).astype(jnp.float32)
    length = values.shape[0]
    summed = jnp.zeros((length, values.shape[1]), jnp.float32)
    for offset in range(tap_weights.shape[0]):
        summed = (
            summed + tap_weights[offset].astype(jnp.float32) * extended[offset : offset + length]
        )
    return summed


def linear_step(first_pair, second_pair):
    return (first_pair[0] * second_pair[0], second_pair[0] * first_pair[1] + second_pair[1])


def shards(
    tokens,
    input_norm_gain,
    output_gate_weight,
    value_input_weight,
    recurrence_input_weight,
    convolution_filter,
    recurrence_filter,
    recurrence_gate_matrix,
    input_gate_matrix,
    channel_decay_rate,
    head_log_decay_add,
    initial_state,
    output_matrix,
):
    token_rows = tokens.astype(jnp.float32)
    inverse_rms = lax.rsqrt(jnp.mean(token_rows * token_rows, axis=1, keepdims=True) + NORM_EPS)
    normed = (token_rows * inverse_rms * input_norm_gain.astype(jnp.float32)).astype(jnp.bfloat16)
    channel_count = output_gate_weight.shape[1]
    weights = (
        lax.all_gather(output_gate_weight, "sp", axis=0, tiled=True),
        lax.all_gather(value_input_weight, "sp", axis=0, tiled=True),
        lax.all_gather(recurrence_input_weight, "sp", axis=0, tiled=True),
    )
    row_block = lax.all_gather(normed, "tp", axis=0, tiled=True)
    projected = jnp.concatenate(
        [
            jnp.dot(row_block, weight, preferred_element_type=jnp.float32).astype(jnp.bfloat16)
            for weight in weights
        ],
        axis=1,
    )
    gate_proj = projected[:, :channel_count]
    value_proj = projected[:, channel_count : 2 * channel_count]
    recur_proj = projected[:, 2 * channel_count :]
    value_tail, recur_tail = shifted(
        (
            value_proj[-(convolution_filter.shape[0] - 1) :],
            recur_proj[-(recurrence_filter.shape[0] - 1) :],
        ),
        "sp",
        1,
    )
    conv_mix = gate_proj.astype(jnp.float32) * causal_taps(
        value_proj, value_tail, convolution_filter
    )
    recur_in = causal_taps(recur_proj, recur_tail, recurrence_filter).astype(jnp.bfloat16)
    length = recur_in.shape[0]
    number_of_heads = recurrence_gate_matrix.shape[0]
    head_width = channel_count // number_of_heads
    grouped = recur_in.reshape(length, number_of_heads, head_width)
    forget_gate = jax.nn.sigmoid(
        jnp.einsum(
            "thi,hij->thj", grouped, recurrence_gate_matrix, preferred_element_type=jnp.float32
        ).reshape(length, channel_count)
    )
    admit_gate = jax.nn.sigmoid(
        jnp.einsum(
            "thi,hij->thj", grouped, input_gate_matrix, preferred_element_type=jnp.float32
        ).reshape(length, channel_count)
    )
    decay_add_rows = jnp.repeat(head_log_decay_add.T, head_width, axis=1)
    logarithm_decay = -DECAY_MULTIPLIER * forget_gate * channel_decay_rate[None, :] + decay_add_rows
    decay_step = jnp.exp(logarithm_decay)
    drive_term = (
        recur_in.astype(jnp.float32) * admit_gate * jnp.sqrt(-jnp.expm1(2.0 * logarithm_decay))
    )
    cum_decay, local_state = lax.associative_scan(linear_step, (decay_step, drive_term), axis=0)
    block_log = jnp.sum(logarithm_decay, axis=0)
    block_end = local_state[-1]
    all_logs, all_ends = (
        lax.all_gather(block_log[None, :], "sp", axis=0, tiled=True),
        lax.all_gather(block_end[None, :], "sp", axis=0, tiled=True),
    )
    devices = all_logs.shape[0]
    position = lax.axis_index("sp")
    earlier = (jnp.arange(devices, dtype=jnp.int32) < position)[:, None]
    masked_logs = jnp.where(earlier, all_logs, 0.0)
    through = jnp.cumsum(masked_logs, axis=0)
    prior_log = jnp.sum(masked_logs, axis=0)
    weights_back = jnp.where(earlier, jnp.exp(jnp.minimum(prior_log[None, :] - through, 0.0)), 0.0)
    incoming = jnp.exp(prior_log) * initial_state + jnp.sum(weights_back * all_ends, axis=0)
    hidden = local_state + cum_decay * incoming[None, :]
    merged = (conv_mix + hidden).astype(jnp.bfloat16)
    contract = (((1,), (1,)), ((), ()))
    return lax.psum_scatter(
        lax.dot_general(merged, output_matrix, contract, preferred_element_type=jnp.float32).astype(
            jnp.bfloat16
        ),
        "tp",
        scatter_dimension=0,
        tiled=True,
    )


def solution(mesh):
    placed = (
        P(("sp", "tp"), None),
        P(),
        P("sp", "tp"),
        P("sp", "tp"),
        P("sp", "tp"),
        P(None, "tp"),
        P(None, "tp"),
        P("tp", None, None),
        P("tp", None, None),
        P("tp"),
        P("tp", "sp"),
        P("tp"),
        P(None, "tp"),
    )
    return jax.shard_map(
        shards, mesh=mesh, in_specs=placed, out_specs=P(("sp", "tp"), None), check_vma=False
    )
```

profile of v0, /device:TPU:0, one launch (start us, length us, event | category | flops | bytes accessed | tf_op | source)
XLA Modules:
  0.0 281.9 jit_solution(6480056698027380360)
XLA Ops:
  8.6 1.9 fusion.12
  14.0 19.0 %all-gather.7.cloned.1.call-done = bf16[384,2048]{1,0:T(8,128)(2,1)} async-done(((bf16[96,2048]{1,0:T(8,128)(2,1)}), bf16[384,2048]{1,0:T(8,128)(2,1)}) %all-gather.7.cloned.1.call-update) | async-done | bytes 1572880 | tf_op jit(solution)/shard_map/all_gather | solution.py:55
  33.1 51.2 %all-gather.11.cloned.1.call-done = bf16[2048,512]{1,0:T(8,128)(2,1)} async-done(((bf16[256,512]{1,0:T(8,128)(2,1)}), bf16[2048,512]{1,0:T(8,128)(2,1)}) %all-gather.11.cloned.1.call-update) | async-done | bytes 2097168 | tf_op jit(solution)/shard_map/all_gather | solution.py:52
  84.3 3.0 %convolution_convert_fusion.2 = bf16[384,512]{1,0:T(8,128)(2,1)S(1)} fusion(bf16[384,2048]{1,0:T(8,128)(2,1)} %all-gather.7.cloned.1.call-done, bf16[2048,512]{1,0:T(8,128)(2,1)} %all-gather.11.cloned.1.call-done), kind=kOutput, calls=%fused_computation.10 | convolution fusion | flops 805502976 | bytes 4063232 | tf_op jit(solution)/shard_map/dot_general | solution.py:58
  87.4 2.5 collective-permute-start
  89.8 44.3 %all-gather.13.cloned.1.call-done = bf16[2048,512]{1,0:T(8,128)(2,1)} async-done(((bf16[256,512]{1,0:T(8,128)(2,1)}), bf16[2048,512]{1,0:T(8,128)(2,1)}) %all-gather.13.cloned.1.call-update) | async-done | bytes 2097168 | tf_op jit(solution)/shard_map/all_gather | solution.py:53
  134.1 3.0 %convolution_convert_fusion.1 = bf16[384,512]{1,0:T(8,128)(2,1)S(1)} fusion(bf16[384,2048]{1,0:T(8,128)(2,1)} %all-gather.7.cloned.1.call-done, bf16[2048,512]{1,0:T(8,128)(2,1)} %all-gather.13.cloned.1.call-done), kind=kOutput, calls=%fused_computation.9 | convolution fusion | flops 805502976 | bytes 4063232 | tf_op jit(solution)/shard_map/dot_general | solution.py:58
  137.1 2.5 collective-permute-start.1
  142.9 2.3 copy.30
  145.2 2.3 fusion.22
  147.5 2.3 copy.31
  149.8 3.4 %sqrt_multiply_fusion = (f32[384,512]{1,0:T(8,128)S(1)}, f32[384,512]{1,0:T(8,128)}) fusion(f32[384,512]{1,0:T(8,128)} %copy.30, f32[384,512]{1,0:T(8,128)} %copy.32, f32[384,512]{1,0:T(8,128)} %copy.31, f32[512]{0:T(512)S(1)} %broadcast_multiply_fusion, f32[387,512]{1,0:T(8,128)S(1)} %maximum_convert_fusion.1, f32[512]{0:T(512)S(1)} %bitcast.56, ...), kind=kLoop, calls=%fused_computation.41 | loop fusion | flops 2949120 | bytes 7088128 | tf_op jit(solution)/shard_map/mul | solution.py:96
  154.2 3.2 %slice.363 = f32[191,512]{1,0:T(8,128)} slice(f32[384,512]{1,0:T(8,128)} %copy-done.2), slice={[2:384:2], [0:512:1]} | slice | bytes 782336 | tf_op jit(solution)/shard_map/slice | solution.py:98
  157.3 2.1 slice.307
  159.4 3.2 %slice.306 = f32[192,512]{1,0:T(8,128)} slice(f32[384,512]{1,0:T(8,128)} %copy-done.2), slice={[0:383:2], [0:512:1]} | slice | bytes 786432 | tf_op jit(solution)/shard_map/slice | solution.py:98
  172.1 27.3 %all-gather = f32[8,1,512]{2,1,0:T(1,128)S(1)} all-gather(f32[1,1,512]{2,1,0:T(1,128)S(1)} %reshape.51), channel_id=1, replica_groups=mesh['sp'=8,'tp'=4] {'sp'}, dimensions={0}, use_global_device_ids=true | all-gather | bytes 18432 | tf_op jit(solution)/shard_map/all_gather | solution.py:102
  203.1 2.5 pad.127
  205.6 1.9 add.261
  209.4 1.9 pad.112
  211.3 2.9 %pad.113 = f32[384,512]{1,0:T(8,128)} pad(f32[192,512]{1,0:T(8,128)} %add.252, f32[]{:T(128)} %constant.8.clone.1), padding=1_0_1x0_0_0 | pad | bytes 1179652 | tf_op jit(solution)/shard_map/pad | solution.py:98
  214.3 2.0 pad.128
  217.1 26.1 %all-gather.1 = f32[8,1,512]{2,1,0:T(1,128)S(1)} all-gather(f32[1,1,512]{2,1,0:T(1,128)S(1)} %add_bitcast_fusion), channel_id=1, replica_groups=mesh['sp'=8,'tp'=4] {'sp'}, dimensions={0}, use_global_device_ids=true | all-gather | bytes 18432 | tf_op jit(solution)/shard_map/all_gather | solution.py:103
  243.3 6.7 %convolution_convert_fusion = bf16[384,2048]{1,0:T(8,128)(2,1)} fusion(bf16[2048,512]{1,0:T(8,128)(2,1)S(1)} %copy-done, bf16[384,2048]{1,0:T(8,128)(2,1)} %all-gather.7.cloned.1.call-done, bf16[2048,512]{1,0:T(8,128)(2,1)} %all-gather.9.cloned.1.call-done, f32[386,512]{1,0:T(8,128)} %maximum_convert_fusion, f32[384,512]{1,0:T(8,128)} %pad.128, ...), kind=kOutput, calls=%fused_computation | convolution fusion | flops 1614151680 | bytes 12853248 | tf_op jit(solution)/shard_map/dot_general | solution.py:117
  250.1 25.3 %reduce-scatter.2.cloned.1.call-done = bf16[96,2048]{1,0:T(8,128)(2,1)} async-done(((bf16[384,2048]{1,0:T(8,128)(2,1)}), bf16[96,2048]{1,0:T(8,128)(2,1)}) %reduce-scatter.2.cloned.1.call-update) | async-done | bytes 393232 | tf_op jit(solution)/shard_map/reduce_scatter | solution.py:116
  (184 shorter events, 25.2 us)
Async XLA Ops:
  6.5 236.8 %copy-start = (bf16[2048,512]{1,0:T(8,128)(2,1)S(1)}, bf16[2048,512]{1,0:T(8,128)(2,1)}, u32[]{:S(2)}) copy-start(bf16[2048,512]{1,0:T(8,128)(2,1)} %param.25) | copy-start | bytes 6291460
  6.5 6.1 %copy-start.11 = (f32[512]{0:T(512)S(1)}, f32[512]{0:T(512)}, u32[]{:S(2)}) copy-start(f32[512]{0:T(512)} %param.22) | copy-start | bytes 6148
  6.5 6.2 %copy-start.9 = (bf16[3,512]{1,0:T(4,128)(2,1)S(1)}, bf16[3,512]{1,0:T(4,128)(2,1)}, u32[]{:S(2)}) copy-start(bf16[3,512]{1,0:T(4,128)(2,1)} %param.18) | copy-start | bytes 9220
  6.5 6.2 %copy-start.8 = (bf16[4,512]{1,0:T(4,128)(2,1)S(1)}, bf16[4,512]{1,0:T(4,128)(2,1)}, u32[]{:S(2)}) copy-start(bf16[4,512]{1,0:T(4,128)(2,1)} %param.19) | copy-start | bytes 12292
  6.5 6.2 %copy-start.10 = (f32[2,384]{1,0:T(2,128)S(1)}, f32[2,384]{1,0:T(2,128)}, u32[]{:S(2)}) copy-start(f32[2,384]{1,0:T(2,128)} %param.23) | copy-start | bytes 9220
  6.5 26.5 %all-gather.7.cloned.1.call-start = ((), (), s32[]{:S(2)}) async-start(), calls=%async_computation.1 | async-start | bytes 1966080 | tf_op jit(solution)/shard_map/all_gather | solution.py:55
  10.5 73.8 %all-gather.11.cloned.1.call-start = ((), (), s32[]{:S(2)}) async-start(), calls=%async_computation.3 | async-start | bytes 2359296 | tf_op jit(solution)/shard_map/all_gather | solution.py:52
  11.3 122.8 %all-gather.13.cloned.1.call-start = ((), (), s32[]{:S(2)}) async-start(), calls=%async_computation.4 | async-start | bytes 2359296 | tf_op jit(solution)/shard_map/all_gather | solution.py:53
  12.0 231.3 %all-gather.9.cloned.1.call-start = ((), (), s32[]{:S(2)}) async-start(), calls=%async_computation.2 | async-start | bytes 2359296 | tf_op jit(solution)/shard_map/all_gather | solution.py:51
  12.6 262.8 %reduce-scatter.2.cloned.1.call-start = ((), (), s32[]{:S(2)}) async-start(), calls=%async_computation.5 | async-start | bytes 1966080 | tf_op jit(solution)/shard_map/reduce_scatter | solution.py:116
  87.4 52.3 %collective-permute-start = (bf16[2,512]{1,0:T(2,128)(2,1)S(1)}, bf16[2,512]{1,0:T(2,128)(2,1)S(1)}, u32[]{:S(2)}, u32[]{:S(2)}) collective-permute-start(bf16[2,512]{1,0:T(2,128)(2,1)S(1)} %slice.380), channel_id=1, source_target_pairs={{0,4},{4,8},{8,12},{12,16},{16,20},{20,24},{24,28},{1,5},{5,9},{9,... | collective-permute-start | bytes 6152 | tf_op jit(solution)/shard_map/ppermute | solution.py:13
  137.1 3.8 %collective-permute-start.1 = (bf16[3,512]{1,0:T(4,128)(2,1)S(1)}, bf16[3,512]{1,0:T(4,128)(2,1)S(1)}, u32[]{:S(2)}, u32[]{:S(2)}) collective-permute-start(bf16[3,512]{1,0:T(4,128)(2,1)S(1)} %slice.384), channel_id=1, source_target_pairs={{0,4},{4,8},{8,12},{12,16},{16,20},{20,24},{24,28},{1,5},{5,9},{9,... | collective-permute-start | bytes 9224 | tf_op jit(solution)/shard_map/ppermute | solution.py:13
  140.6 1.0 copy-start.13
  153.2 0.9 copy-start.2
  153.2 9.4 %copy-start.1 = (f32[384,512]{1,0:T(8,128)S(1)}, f32[384,512]{1,0:T(8,128)}, u32[]{:S(2)}) copy-start(f32[384,512]{1,0:T(8,128)} %get-tuple-element.12) | copy-start | bytes 2359300
  205.6 2.7 copy-start.3
  205.6 2.7 copy-start.4
  205.6 2.7 copy-start.5
  209.4 4.9 %copy-start.6 = (f32[191,512]{1,0:T(8,128)S(1)}, f32[191,512]{1,0:T(8,128)}, u32[]{:S(2)}) copy-start(f32[191,512]{1,0:T(8,128)} %get-tuple-element.14) | copy-start | bytes 1173508
  209.4 6.8 %copy-start.7 = (f32[192,512]{1,0:T(8,128)S(1)}, f32[192,512]{1,0:T(8,128)}, u32[]{:S(2)}) copy-start(f32[192,512]{1,0:T(8,128)} %add.261) | copy-start | bytes 1179652
  211.3 32.0 %copy-start.12 = (f32[512]{0:T(512)S(1)}, f32[512]{0:T(512)}, u32[]{:S(2)}) copy-start(f32[512]{0:T(512)} %param.24) | copy-start | bytes 6148
Sparse Core Ops, SparseCore 0:
  10.7 22.3 all-gather.6
  35.2 49.0 all-gather.10
  86.4 47.6 all-gather.12
  136.1 47.7 all-gather.8
  250.2 25.1 reduce-scatter.1
where the time goes:
time: 283 us; the launch traced here: 282 us
  waiting for transfers between devices  142 us (50%)
  blocking collectives  53.4 us (19%)
  local copies, waits for them, and re-layouts  33 us (12%)
  other arithmetic  17.9 us (6%)
  matrix products  16.4 us (6%)
  between operations  14 us (5%)
  starting transfers between devices  5.12 us (2%)
    all_gather x1, waiting for transfers between devices, shards(): lax.all_gather(value_input_weight, 'sp', axis=0, tiled=True)  51.2 us
    all_gather x1, waiting for transfers between devices, shards(): lax.all_gather(recurrence_input_weight, 'sp', axis=0, tiled=True)  44.3 us
    all_gather x1, blocking collectives, shards(): lax.all_gather(block_log[None, :], 'sp', axis=0, tiled=True)  27.3 us
    all_gather x1, blocking collectives, shards(): lax.all_gather(block_end[None, :], 'sp', axis=0, tiled=True)  26.1 us
    reduce_scatter x1, waiting for transfers between devices, shards(): lax.psum_scatter(lax.dot_general(merged, output_matrix, contract, preferr...  25.3 us
    all_gather x1, waiting for transfers between devices, shards(): row_block = lax.all_gather(normed, 'tp', axis=0, tiled=True)  19 us
    slice x56, local copies, waits for them, and re-layouts, shards(): lax.associative_scan(linear_step, (decay_step, drive_term), axis=0)  15.2 us
    pad x30, local copies, waits for them, and re-layouts, shards(): lax.associative_scan(linear_step, (decay_step, drive_term), axis=0)  10.8 us
  transfers between devices with their start and end apart: 7, of which 5 were waited for; matrix products, arithmetic and copies ran while one was open for 20% of the time, Pallas kernels for 0%

commit v1 on v0

--- a/solution.py
+++ b/solution.py
@@ -43,6 +43,22 @@
     initial_state,
     output_matrix,
 ):
+
+    def keep_up_things(original, net_axis="tp"):
+        stack_in = [original]
+        n_blocks = jax.lax.axis_size(net_axis)
+        for pp in range(n_blocks - 1):
+            stack_in.append(
+                jax.lax.ppermute(
+                    stack_in[-1], net_axis, perm=[(i, (i + 1) % n_blocks) for i in range(n_blocks)]
+                )
+            )
+        return jnp.roll(
+            jnp.concatenate(stack_in[::-1], 0),
+            (jax.lax.axis_index(net_axis) + 1) * original.shape[0],
+            0,
+        )
+
     token_rows = tokens.astype(jnp.float32)
     inverse_rms = lax.rsqrt(jnp.mean(token_rows * token_rows, axis=1, keepdims=True) + NORM_EPS)
     normed = (token_rows * inverse_rms * input_norm_gain.astype(jnp.float32)).astype(jnp.bfloat16)
@@ -52,7 +68,7 @@
         lax.all_gather(value_input_weight, "sp", axis=0, tiled=True),
         lax.all_gather(recurrence_input_weight, "sp", axis=0, tiled=True),
     )
-    row_block = lax.all_gather(normed, "tp", axis=0, tiled=True)
+    row_block = keep_up_things(normed)
     projected = jnp.concatenate(
         [
             jnp.dot(row_block, weight, preferred_element_type=jnp.float32).astype(jnp.bfloat16)

time: 283 us -> 338 us (1.19)
  local copies, waits for them, and re-layouts: 33 us -> 99.9 us
  waiting for transfers between devices: 142 us -> 107 us
  other arithmetic: 17.9 us -> 38.7 us
    slice x56, local copies, waits for them, and re-layouts: 15.2 us -> 70.1 us  [shards(): lax.associative_scan(linear_step, (decay_step, drive_term), axis=0)]
    all_gather x1, waiting for transfers between devices: 51.2 us -> 16.7 us  [shards(): lax.all_gather(value_input_weight, 'sp', axis=0, tiled=True)]
    all_gather x1 -> x0, waiting for transfers between devices: 19 us -> none  [shards(): row_block = lax.all_gather(normed, 'tp', axis=0, tiled=True)]
    ppermute x0 -> x3, waiting for transfers between devices: none -> 18.5 us  [keep_up_things(): jax.lax.ppermute(stack_in[-1], net_axis, perm=[(i, (i + 1) % n_blocks) fo...]
    add x15, other arithmetic: 3.68 us -> 16.3 us  [linear_step(): second_pair[0] * first_pair[1] + second_pair[1]]
    unnamed x29 -> x57, local copies, waits for them, and re-layouts: 1.16 us -> 8.76 us
    concatenate x15, other arithmetic: 0.23 us -> 5.51 us  [shards(): lax.associative_scan(linear_step, (decay_step, drive_term), axis=0)]
    pad x30, local copies, waits for them, and re-layouts: 10.8 us -> 14.4 us  [shards(): lax.associative_scan(linear_step, (decay_step, drive_term), axis=0)]
  transfers between devices with their start and end apart: 7 -> 9, of which waited for: 5 -> 7; matrix products, arithmetic and copies ran while one was open for 20% -> 44% of each run, Pallas kernels for 0% -> 0%
where the time goes in v1:
time: 338 us; the launch traced here: 335 us
  waiting for transfers between devices  107 us (32%)
  local copies, waits for them, and re-layouts  99.9 us (30%)
  blocking collectives  53.4 us (16%)
  other arithmetic  38.7 us (11%)
  matrix products  17.2 us (5%)
  between operations  13.8 us (4%)
  starting transfers between devices  5.73 us (2%)
    slice x56, local copies, waits for them, and re-layouts, shards(): lax.associative_scan(linear_step, (decay_step, drive_term), axis=0)  70.1 us
    all_gather x1, waiting for transfers between devices, shards(): lax.all_gather(recurrence_input_weight, 'sp', axis=0, tiled=True)  44.2 us
    all_gather x1, blocking collectives, shards(): lax.all_gather(block_log[None, :], 'sp', axis=0, tiled=True)  27.3 us
    all_gather x1, blocking collectives, shards(): lax.all_gather(block_end[None, :], 'sp', axis=0, tiled=True)  26.1 us
    reduce_scatter x1, waiting for transfers between devices, shards(): lax.psum_scatter(lax.dot_general(merged, output_matrix, contract, preferr...  25.3 us
    ppermute x3, waiting for transfers between devices, keep_up_things(): jax.lax.ppermute(stack_in[-1], net_axis, perm=[(i, (i + 1) % n_blocks) fo...  18.5 us
    all_gather x1, waiting for transfers between devices, shards(): lax.all_gather(value_input_weight, 'sp', axis=0, tiled=True)  16.7 us
    add x15, other arithmetic, linear_step(): second_pair[0] * first_pair[1] + second_pair[1]  16.3 us
  transfers between devices with their start and end apart: 9, of which 7 were waited for; matrix products, arithmetic and copies ran while one was open for 44% of the time, Pallas kernels for 0%

profile of v1, /device:TPU:0, one launch (start us, length us, event | category | flops | bytes accessed | tf_op | source)
XLA Modules:
  0.0 335.2 jit_solution(9580102540912084040)
XLA Ops:
  11.7 7.5 %collective-permute-done = bf16[96,2048]{1,0:T(8,128)(2,1)} collective-permute-done((bf16[96,2048]{1,0:T(8,128)(2,1)S(1)}, bf16[96,2048]{1,0:T(8,128)(2,1)}, u32[]{:S(2)}, u32[]{:S(2)}) %collective-permute-start) | collective-permute-done | bytes 393248 | tf_op jit(solution)/shard_map/ppermute | solution.py:52
  22.4 4.3 %collective-permute-done.1 = bf16[96,2048]{1,0:T(8,128)(2,1)} collective-permute-done((bf16[96,2048]{1,0:T(8,128)(2,1)}, bf16[96,2048]{1,0:T(8,128)(2,1)}, u32[]{:S(2)}, u32[]{:S(2)}) %collective-permute-start.1) | collective-permute-done | bytes 393248 | tf_op jit(solution)/shard_map/ppermute | solution.py:52
  27.3 6.8 %collective-permute-done.2 = bf16[96,2048]{1,0:T(8,128)(2,1)S(1)} collective-permute-done((bf16[96,2048]{1,0:T(8,128)(2,1)}, bf16[96,2048]{1,0:T(8,128)(2,1)S(1)}, u32[]{:S(2)}, u32[]{:S(2)}) %collective-permute-start.2) | collective-permute-done | bytes 393248 | tf_op jit(solution)/shard_map/ppermute | solution.py:52
  44.6 16.7 %all-gather.8.cloned.1.call-done = bf16[2048,512]{1,0:T(8,128)(2,1)} async-done(((bf16[256,512]{1,0:T(8,128)(2,1)}), bf16[2048,512]{1,0:T(8,128)(2,1)}) %all-gather.8.cloned.1.call-update) | async-done | bytes 2097168 | tf_op jit(solution)/shard_map/all_gather | solution.py:68
  61.3 3.1 convolution_convert_fusion.2
  64.4 2.5 collective-permute-start.3
  66.9 44.2 %all-gather.10.cloned.1.call-done = bf16[2048,512]{1,0:T(8,128)(2,1)} async-done(((bf16[256,512]{1,0:T(8,128)(2,1)}), bf16[2048,512]{1,0:T(8,128)(2,1)}) %all-gather.10.cloned.1.call-update) | async-done | bytes 2097168 | tf_op jit(solution)/shard_map/all_gather | solution.py:69
  111.1 3.1 convolution_convert_fusion.1
  114.2 2.6 collective-permute-start.4
  120.5 2.3 copy.31
  122.8 2.3 fusion.5
  125.0 2.3 copy.30
  127.4 3.7 %sqrt_multiply_fusion = (f32[384,512]{1,0:T(8,128)}, f32[384,512]{1,0:T(8,128)}) fusion(f32[384,512]{1,0:T(8,128)} %copy.30, f32[384,512]{1,0:T(8,128)} %copy.32, f32[384,512]{1,0:T(8,128)} %copy.31, f32[512]{0:T(512)S(1)} %broadcast_multiply_fusion, f32[387,512]{1,0:T(8,128)S(1)} %maximum_convert_fusion.1, f32[512]{0:T(512)S(1)} %bitcast.53, ...), kind=kLoop, calls=%fused_computation.44 | loop fusion | flops 2949120 | bytes 7088128 | tf_op jit(solution)/shard_map/mul | solution.py:112
  133.2 3.2 slice.307
  136.4 3.2 slice.305
  139.5 3.1 slice.309
  205.6 3.2 slice.363
  228.6 2.5 pad.127
  232.9 2.2 fusion.34
  237.1 27.3 %all-gather = f32[8,1,512]{2,1,0:T(1,128)S(1)} all-gather(f32[1,1,512]{2,1,0:T(1,128)S(1)} %reshape.51), channel_id=1, replica_groups=mesh['sp'=8,'tp'=4] {'sp'}, dimensions={0}, use_global_device_ids=true | all-gather | bytes 18432 | tf_op jit(solution)/shard_map/all_gather | solution.py:118
  264.5 2.9 pad.129
  270.1 26.1 %all-gather.1 = f32[8,1,512]{2,1,0:T(1,128)S(1)} all-gather(f32[1,1,512]{2,1,0:T(1,128)S(1)} %add_bitcast_fusion), channel_id=1, replica_groups=mesh['sp'=8,'tp'=4] {'sp'}, dimensions={0}, use_global_device_ids=true | all-gather | bytes 18432 | tf_op jit(solution)/shard_map/all_gather | solution.py:119
  296.4 7.0 %convolution_convert_fusion = bf16[384,2048]{1,0:T(8,128)(2,1)} fusion(bf16[2048,512]{1,0:T(8,128)(2,1)S(1)} %copy-done, bf16[2048,512]{1,0:T(8,128)(2,1)} %all-gather.6.cloned.1.call-done, bf16[768,2048]{1,0:T(8,128)(2,1)} %constant_dynamic-update-slice_fusion, s32[]{:T(128)S(6)} %select_n.21, f32[386,512]{1,0:T(8,128)} %maximum_convert_fusion, ...), kind=kOutput, calls=%fused_computation | convolution fusion | flops 1614151680 | bytes 12853252 | tf_op jit(solution)/shard_map/dot_general | solution.py:133
  303.4 25.3 %reduce-scatter.2.cloned.1.call-done = bf16[96,2048]{1,0:T(8,128)(2,1)} async-done(((bf16[384,2048]{1,0:T(8,128)(2,1)}), bf16[96,2048]{1,0:T(8,128)(2,1)}) %reduce-scatter.2.cloned.1.call-update) | async-done | bytes 393232 | tf_op jit(solution)/shard_map/reduce_scatter | solution.py:132
  (217 shorter events, 114.2 us)
Async XLA Ops:
  6.5 289.8 %copy-start = (bf16[2048,512]{1,0:T(8,128)(2,1)S(1)}, bf16[2048,512]{1,0:T(8,128)(2,1)}, u32[]{:S(2)}) copy-start(bf16[2048,512]{1,0:T(8,128)(2,1)} %param.25) | copy-start | bytes 6291460
  6.5 20.2 %copy-start.10 = (bf16[3,512]{1,0:T(4,128)(2,1)S(1)}, bf16[3,512]{1,0:T(4,128)(2,1)}, u32[]{:S(2)}) copy-start(bf16[3,512]{1,0:T(4,128)(2,1)} %param.18) | copy-start | bytes 9220
  6.5 20.8 %copy-start.9 = (bf16[4,512]{1,0:T(4,128)(2,1)S(1)}, bf16[4,512]{1,0:T(4,128)(2,1)}, u32[]{:S(2)}) copy-start(bf16[4,512]{1,0:T(4,128)(2,1)} %param.19) | copy-start | bytes 12292
  6.5 54.8 %all-gather.8.cloned.1.call-start = ((), (), s32[]{:S(2)}) async-start(), calls=%async_computation.2 | async-start | bytes 2359296 | tf_op jit(solution)/shard_map/all_gather | solution.py:68
  7.3 103.8 %all-gather.10.cloned.1.call-start = ((), (), s32[]{:S(2)}) async-start(), calls=%async_computation.3 | async-start | bytes 2359296 | tf_op jit(solution)/shard_map/all_gather | solution.py:69
  8.0 30.4 %copy-start.1 = (bf16[96,2048]{1,0:T(8,128)(2,1)S(1)}, bf16[96,2048]{1,0:T(8,128)(2,1)}, u32[]{:S(2)}) copy-start(bf16[96,2048]{1,0:T(8,128)(2,1)} %param.13) | copy-start | bytes 1179652
  8.0 288.3 %all-gather.6.cloned.1.call-start = ((), (), s32[]{:S(2)}) async-start(), calls=%async_computation.1 | async-start | bytes 2359296 | tf_op jit(solution)/shard_map/all_gather | solution.py:67
  11.2 8.0 %collective-permute-start = (bf16[96,2048]{1,0:T(8,128)(2,1)S(1)}, bf16[96,2048]{1,0:T(8,128)(2,1)}, u32[]{:S(2)}, u32[]{:S(2)}) collective-permute-start(bf16[96,2048]{1,0:T(8,128)(2,1)S(1)} %fusion.17), channel_id=1, source_target_pairs={{0,1},{1,2},{2,3},{3,0},{4,5},{5,6},{6,7},{7,4},{8,9},{9,10},{10,1... | collective-permute-start | bytes 1179656 | tf_op jit(solution)/shard_map/ppermute | solution.py:52
  19.2 7.5 %collective-permute-start.1 = (bf16[96,2048]{1,0:T(8,128)(2,1)}, bf16[96,2048]{1,0:T(8,128)(2,1)}, u32[]{:S(2)}, u32[]{:S(2)}) collective-permute-start(bf16[96,2048]{1,0:T(8,128)(2,1)} %collective-permute-done), channel_id=1, source_target_pairs={{0,1},{1,2},{2,3},{3,0},{4,5},{5,6},{6,7},{7,4},{8,9},{9,10},{10,1... | collective-permute-start | bytes 1179656 | tf_op jit(solution)/shard_map/ppermute | solution.py:52
  19.2 309.5 %reduce-scatter.2.cloned.1.call-start = ((), (), s32[]{:S(2)}) async-start(), calls=%async_computation.4 | async-start | bytes 1966080 | tf_op jit(solution)/shard_map/reduce_scatter | solution.py:132
  26.7 7.4 %collective-permute-start.2 = (bf16[96,2048]{1,0:T(8,128)(2,1)}, bf16[96,2048]{1,0:T(8,128)(2,1)S(1)}, u32[]{:S(2)}, u32[]{:S(2)}) collective-permute-start(bf16[96,2048]{1,0:T(8,128)(2,1)} %collective-permute-done.1), channel_id=1, source_target_pairs={{0,1},{1,2},{2,3},{3,0},{4,5},{5,6},{6,7},{7,4},{8,9},{9,10},{10,1... | collective-permute-start | bytes 1179656 | tf_op jit(solution)/shard_map/ppermute | solution.py:52
  64.4 52.4 %collective-permute-start.3 = (bf16[2,512]{1,0:T(2,128)(2,1)S(1)}, bf16[2,512]{1,0:T(2,128)(2,1)S(1)}, u32[]{:S(2)}, u32[]{:S(2)}) collective-permute-start(bf16[2,512]{1,0:T(2,128)(2,1)S(1)} %slice.380), channel_id=1, source_target_pairs={{0,4},{4,8},{8,12},{12,16},{16,20},{20,24},{24,28},{1,5},{5,9},{9,... | collective-permute-start | bytes 6152 | tf_op jit(solution)/shard_map/ppermute | solution.py:13
  114.2 3.9 %collective-permute-start.4 = (bf16[3,512]{1,0:T(4,128)(2,1)S(1)}, bf16[3,512]{1,0:T(4,128)(2,1)S(1)}, u32[]{:S(2)}, u32[]{:S(2)}) collective-permute-start(bf16[3,512]{1,0:T(4,128)(2,1)S(1)} %slice.384), channel_id=1, source_target_pairs={{0,4},{4,8},{8,12},{12,16},{16,20},{20,24},{24,28},{1,5},{5,9},{9,... | collective-permute-start | bytes 9224 | tf_op jit(solution)/shard_map/ppermute | solution.py:13
  145.6 58.5 %copy-start.2 = (f32[384,512]{1,0:T(8,128)S(1)}, f32[384,512]{1,0:T(8,128)}, u32[]{:S(2)}) copy-start(f32[384,512]{1,0:T(8,128)} %get-tuple-element.12) | copy-start | bytes 2359300
  204.1 12.7 %copy-start.16 = (f32[1,512]{1,0:T(1,128)S(1)}, f32[1,512]{1,0:T(1,128)}, u32[]{:S(2)}) copy-start(f32[1,512]{1,0:T(1,128)} %slice.393) | copy-start | bytes 6148
  210.6 9.1 %copy-start.7 = (f32[47,512]{1,0:T(8,128)S(1)}, f32[47,512]{1,0:T(8,128)}, u32[]{:S(2)}) copy-start(f32[47,512]{1,0:T(8,128)} %slice.316) | copy-start | bytes 288772
  210.6 9.1 %copy-start.8 = (f32[47,512]{1,0:T(8,128)S(1)}, f32[47,512]{1,0:T(8,128)}, u32[]{:S(2)}) copy-start(f32[47,512]{1,0:T(8,128)} %slice.359) | copy-start | bytes 288772
  231.1 33.3 %copy-start.18 = (pred[8]{0:T(512)(128)(4,1)S(1)}, pred[8]{0:T(512)(128)(4,1)}, u32[]{:S(2)}) copy-start(pred[8]{0:T(512)(128)(4,1)} %iota_compare_fusion) | copy-start | bytes 28
  232.9 34.5 %copy-start.11 = (f32[1,512]{1,0:T(1,128)S(1)}, f32[1,512]{1,0:T(1,128)}, u32[]{:S(2)}) copy-start(f32[1,512]{1,0:T(1,128)} %slice.415) | copy-start | bytes 6148
  235.1 32.3 %copy-start.4 = (f32[191,512]{1,0:T(8,128)S(1)}, f32[191,512]{1,0:T(8,128)}, u32[]{:S(2)}) copy-start(f32[191,512]{1,0:T(8,128)} %get-tuple-element.14) | copy-start | bytes 1173508
  235.1 61.1 %copy-start.20 = (f32[512]{0:T(512)S(1)}, f32[512]{0:T(512)}, u32[]{:S(2)}) copy-start(f32[512]{0:T(512)} %param.24) | copy-start | bytes 6148
  235.1 61.2 %copy-start.21 = (f32[1,512]{1,0:T(1,128)S(1)}, f32[1,512]{1,0:T(1,128)}, u32[]{:S(2)}) copy-start(f32[1,512]{1,0:T(1,128)} %get-tuple-element.43) | copy-start | bytes 6148
  235.1 61.2 %copy-start.22 = (f32[1,512]{1,0:T(1,128)S(1)}, f32[1,512]{1,0:T(1,128)}, u32[]{:S(2)}) copy-start(f32[1,512]{1,0:T(1,128)} %get-tuple-element.44) | copy-start | bytes 6148
  235.1 61.2 %copy-start.23 = (f32[1,512]{1,0:T(1,128)S(1)}, f32[1,512]{1,0:T(1,128)}, u32[]{:S(2)}) copy-start(f32[1,512]{1,0:T(1,128)} %get-tuple-element.45) | copy-start | bytes 6148
  (10 other events, 49.4 us)
Sparse Core Ops, SparseCore 0:
  9.5 51.7 all-gather.7
  63.4 47.6 all-gather.9
  113.2 47.6 all-gather.5
  303.5 25.1 reduce-scatter.1
